TPU v7x, 256 devices: a whole 4x4x8 slice. The times are simulated.
256 devices in a mesh: dp: 4 (over x), kv: 32 (over z, y), tp: 2 (over core).
Axes of the slice: x: 4, y: 4, z: 8, core: 2. Of those that a mesh axis runs over, the one named last changes fastest.
Arguments:
- tokens: bfloat16 [32, 4096], P('dp', 'kv'), may hold values from -6 to 6
- token_gain: float32 [4096], P('kv'), may hold values from 0.1 to 1.9
- asker_narrow_matrix: bfloat16 [4096, 1536], P('kv'), may hold values from -0.09375 to 0.09375
- hidden_narrow_matrix: bfloat16 [4096, 1088], P('kv'), may hold values from -0.09375 to 0.09375
- asker_multiplier: float32 [1536], replicated, may hold values from 0.1 to 1.9
- hidden_multiplier: float32 [1024], replicated, may hold values from 0.1 to 1.9
- asker_unspun_matrix: bfloat16 [1536, 64, 128], P(None, ('kv', 'tp')), may hold values from -0.15625 to 0.15625
- asker_spin_matrix: bfloat16 [1536, 64, 64], P(None, ('kv', 'tp')), may hold values from -0.15625 to 0.15625
- lock_widen_matrix: bfloat16 [64, 128, 1024], P(('kv', 'tp')), may hold values from -0.25 to 0.25
- payload_widen_matrix: bfloat16 [64, 1024, 128], P(('kv', 'tp')), may hold values from -0.75 to 0.75
- w_output: bfloat16 [8192, 4096], P(('kv', 'tp')), may hold values from -1.5 to 1.5
- cache_latent: bfloat16 [32, 8192, 1024], P('dp', 'kv'), may hold values from -4 to 4
- cache_rotary: bfloat16 [32, 8192, 64], P('dp', 'kv'), may hold values from -400 to 400
- lengths: int32 [32], P('dp'), may hold values from 4096 to 8191, as said below
Outputs:
- attention_out: float32 [32, 4096], P('dp', ('kv', 'tp'))
- incoming_hidden: float32 [32, 1024], P('dp')
- incoming_spun: float32 [32, 64], P('dp')
Inputs may be any that keep to these rules, and one draw needn't show every extreme that they name: `lengths`: each length lies in 4096 to 8191; some sequence has 8191 and some has 4096.
All inputs are finite; a program needn't handle non-finite values.
Results may differ from a plain program's by a relative error of at most 0.015.
Values may be sent and summed in bfloat16 or wider, within the bound.
A program may use at most 64 MiB of HBM per device.

v0:
```python
import math

import jax
import jax.numpy as jnp
from jax import lax
from jax.sharding import PartitionSpec as P

MODEL_BREADTH = 4096


EPS = 1e-06
THETA = 10000.0


def copy_for_each(array, axis):
    devices = lax.axis_size(axis)
    return lax.all_to_all(
        jnp.broadcast_to(array[None], (devices, *array.shape)), axis, 0, 0, tiled=True
    )


def over_copies(array, axis):
    everything = copy_for_each(array, axis)
    return jnp.sum(everything, axis=0)


def together(arrays, axis):
    ends = [0]
    for a in arrays:
        ends.append(ends[-1] + a.size)
    total = over_copies(jnp.concatenate([a.ravel() for a in arrays]), axis)
    return tuple((total[b:e].reshape(a.shape) for a, b, e in zip(arrays, ends, ends[1:])))


def sent_together(arrays, axis, dim, along):
    widths = [a.shape[along] for a in arrays]
    both = jnp.concatenate(arrays, axis=along)
    filled = lax.all_gather(both, axis, axis=dim, tiled=True)
    return tuple(jnp.split(filled, [sum(widths[:k]) for k in range(1, len(widths))], axis=along))


def in_one_piece(arrays, axis, split_dim, concat_dim, along):
    widths = [math.prod(a.shape[along:]) for a in arrays]
    both = jnp.concatenate(
        [a.reshape(*a.shape[:along], w) for a, w in zip(arrays, widths)], axis=along
    )
    filled = lax.all_to_all(both, axis, split_axis=split_dim, concat_axis=concat_dim, tiled=True)
    parts = jnp.split(filled, [sum(widths[:k]) for k in range(1, len(widths))], axis=along)
    return tuple(
        (b.reshape(*filled.shape[:along], *a.shape[along:]) for a, b in zip(arrays, parts))
    )


def cut_along(array, dim, devices):
    before, after = (array.shape[:dim], array.shape[dim + 1 :])
    return jnp.moveaxis(array.reshape(*before, devices, -1, *after), dim, 0)


def sum_at_owner(array, axis, dim):
    devices = lax.axis_size(axis)
    parts = lax.all_to_all(cut_along(array, dim, devices), axis, 0, 0, tiled=True)
    return jnp.sum(parts, axis=0)


def magnitude_divisor(values, gain):
    mean_square = jnp.mean(values * values, axis=-1, keepdims=True)
    return values * lax.rsqrt(mean_square + EPS) * gain


def spinning(values, position):
    half_width = values.shape[-1] // 2
    exponent = jnp.arange(half_width, dtype=jnp.float32) * (2.0 / values.shape[-1])
    frequency = THETA ** (-exponent)
    angles = position.astype(jnp.float32)[:, None] * frequency[None, :]
    angles = angles.reshape((angles.shape[0],) + (1,) * (values.ndim - 2) + (half_width,))
    cosine = jnp.cos(angles)
    sine_table = jnp.sin(angles)
    former = values[..., :half_width]
    latter = values[..., half_width:]
    return jnp.concatenate(
        [former * cosine - latter * sine_table, former * sine_table + latter * cosine], axis=-1
    )


def local(
    tokens,
    token_gain,
    asker_narrow_matrix,
    hidden_narrow_matrix,
    asker_multiplier,
    hidden_multiplier,
    asker_unspun_matrix,
    asker_spin_matrix,
    lock_widen_matrix,
    payload_widen_matrix,
    w_output,
    cache_latent,
    cache_rotary,
    lengths,
):
    tokens_wide = tokens.astype(jnp.float32)
    squares = jnp.sum(tokens_wide * tokens_wide, axis=1, keepdims=True)
    scaled = (tokens_wide * token_gain).astype(jnp.bfloat16)
    query_part = jnp.dot(scaled, asker_narrow_matrix, preferred_element_type=jnp.float32)
    latent_part = jnp.dot(scaled, hidden_narrow_matrix, preferred_element_type=jnp.float32)
    squares, query_down, hidden_squeeze = together((squares, query_part, latent_part), "kv")
    row_scale = lax.rsqrt(squares / MODEL_BREADTH + EPS)
    query_down = query_down * row_scale
    hidden_squeeze = hidden_squeeze * row_scale
    seqs_here, query_width = query_down.shape
    latent_width = lock_widen_matrix.shape[2]
    own_heads = asker_unspun_matrix.shape[1]
    nope_width = asker_unspun_matrix.shape[2]
    rope_width = asker_spin_matrix.shape[2]
    value_width = payload_widen_matrix.shape[2]
    squeezed = magnitude_divisor(query_down, asker_multiplier).astype(jnp.bfloat16)
    incoming_hidden = magnitude_divisor(hidden_squeeze[:, :latent_width], hidden_multiplier)
    incoming_spun = spinning(hidden_squeeze[:, latent_width:], lengths)
    fresh_hidden = incoming_hidden.astype(jnp.bfloat16)
    fresh_spun = incoming_spun.astype(jnp.bfloat16)
    asker_unspun = jnp.dot(
        squeezed,
        asker_unspun_matrix.reshape(query_width, own_heads * nope_width),
        preferred_element_type=jnp.float32,
    )
    asker_unspun = asker_unspun.reshape(seqs_here, own_heads, nope_width).astype(jnp.bfloat16)
    query_latent = jnp.einsum(
        "shd,hdc->shc", asker_unspun, lock_widen_matrix, preferred_element_type=jnp.float32
    ).astype(jnp.bfloat16)
    asker_spun = jnp.dot(
        squeezed,
        asker_spin_matrix.reshape(query_width, own_heads * rope_width),
        preferred_element_type=jnp.float32,
    )
    asker_spun = spinning(asker_spun.reshape(seqs_here, own_heads, rope_width), lengths).astype(
        jnp.bfloat16
    )
    all_latent, all_turned = sent_together((query_latent, asker_spun), "kv", 1, 2)
    span = cache_latent.shape[1]
    positions = lax.axis_index("kv") * span + jnp.arange(span, dtype=jnp.int32)
    fresh_slot = positions[None, :] == lengths[:, None]
    keys_latent = jnp.where(fresh_slot[:, :, None], fresh_hidden[:, None, :], cache_latent)
    keys_turned = jnp.where(fresh_slot[:, :, None], fresh_spun[:, None, :], cache_rotary)
    visible = (positions[None, :] <= lengths[:, None])[:, None, :]
    scores = jnp.einsum("shc,spc->shp", all_latent, keys_latent, preferred_element_type=jnp.float32)
    scores = scores + jnp.einsum(
        "shr,spr->shp", all_turned, keys_turned, preferred_element_type=jnp.float32
    )
    scores = jnp.where(visible, scores * (nope_width + rope_width) ** (-0.5), -1e30)
    local_max = jnp.max(scores, axis=2)
    weights = jnp.where(visible, jnp.exp(scores - local_max[:, :, None]), 0.0)
    local_total = jnp.sum(weights, axis=2)
    local_mix = jnp.einsum(
        "shp,spc->shc",
        weights.astype(jnp.bfloat16),
        keys_latent,
        preferred_element_type=jnp.float32,
    )
    taken_max, taken_total, taken_mix = in_one_piece(
        (local_max[None], local_total[None], local_mix[None]), "kv", 2, 0, 3
    )
    highest = jnp.max(taken_max, axis=0)
    factor = jnp.exp(taken_max - highest[None])
    denominator = jnp.sum(taken_total * factor, axis=0)
    mixture = jnp.sum(taken_mix * factor[..., None], axis=0)
    attended = (mixture / denominator[:, :, None]).astype(jnp.bfloat16)
    head_values = jnp.einsum(
        "shc,hcv->shv", attended, payload_widen_matrix, preferred_element_type=jnp.float32
    ).astype(jnp.bfloat16)
    flat_values = head_values.reshape(seqs_here, own_heads * value_width)
    summed = sum_at_owner(
        lax.dot_general(
            w_output, flat_values, (((0,), (1,)), ((), ())), preferred_element_type=jnp.float32
        ),
        ("kv", "tp"),
        0,
    )
    return (summed.T, incoming_hidden, incoming_spun)


def solution(mesh):
    return jax.shard_map(
        local,
        mesh=mesh,
        in_specs=(
            P("dp", "kv"),
            P("kv"),
            P("kv", None),
            P("kv", None),
            P(),
            P(),
            P(None, ("kv", "tp"), None),
            P(None, ("kv", "tp"), None),
            P(("kv", "tp"), None, None),
            P(("kv", "tp"), None, None),
            P(("kv", "tp"), None),
            P("dp", "kv", None),
            P("dp", "kv", None),
            P("dp"),
        ),
        out_specs=(P("dp", ("kv", "tp")), P("dp", None), P("dp", None)),
        check_vma=False,
    )
```

profile of v0, /device:TPU:1, one launch (start us, length us, event | category | flops | bytes accessed | tf_op | source)
XLA Modules:
  0.0 199.8 jit_solution(5115843628619939654)
XLA Ops:
  0.6 0.0 copy-start
  0.6 0.9 fusion.39
  1.5 1.2 fusion.52
  2.7 1.2 fusion.50
  3.9 0.1 reshape.408
  4.0 0.0 copy-start.4
  4.0 0.1 concatenate.27
  4.1 0.0 copy-start.6
  4.1 2.9 %broadcast_in_dim.55 = f32[32,1,21000]{2,1,0:T(1,128)} broadcast(f32[21000]{0:T(1024)S(1)} %concatenate.27), dimensions={2} | broadcast | bytes 2772000 | tf_op jit(solution)/shard_map/broadcast_in_dim | solution.py:18
  7.0 12.3 %all-to-all-start = ((f32[32,1,21000]{2,1,0:T(1,128)}), f32[32,1,21000]{2,1,0:T(1,128)}, u32[]{:S(2)}, u32[]{:S(2)}) async-start(f32[32,1,21000]{2,1,0:T(1,128)} %broadcast_in_dim.55), calls=%async_computation | async-start | bytes 5406720 | tf_op jit(solution)/shard_map/all_to_all | solution.py:17
  19.3 0.0 copy-start.5
  19.3 0.0 copy-done.4
  19.4 0.0 copy-done.6
  19.4 0.1 broadcast_compare_fusion.1
  19.5 61.2 %all-to-all-done = f32[32,1,21000]{2,1,0:T(1,128)} async-done(((f32[32,1,21000]{2,1,0:T(1,128)}), f32[32,1,21000]{2,1,0:T(1,128)}, u32[]{:S(2)}, u32[]{:S(2)}) %all-to-all-start) | async-done | bytes 2688032 | tf_op jit(solution)/shard_map/all_to_all | solution.py:17
  80.7 3.3 %reduce_sum.75 = f32[21000]{0:T(1024)S(1)} reduce(f32[32,1,21000]{2,1,0:T(1,128)} %all-to-all-done, f32[]{:T(128)} %constant.8.clone.1), dimensions={0,1}, to_apply=%region_1.0 | reduce | flops 651000 | bytes 2772004 | tf_op jit(solution)/shard_map/reduce_sum | solution.py:24
  84.1 0.1 slice.35
  84.1 0.1 slice.37
  84.2 0.2 multiply_reduce_fusion
  84.4 0.1 mul.216
  84.5 0.1 mul.211
  84.6 0.1 multiply_convert_fusion
  84.7 0.1 convert_element_type.94
  84.8 0.0 copy-done.3
  84.8 0.1 convolution_bitcast_fusion.1
  84.9 0.0 copy-done.1
  84.9 0.0 copy-done.2
  84.9 0.3 fusion.8
  85.2 0.1 fusion.46
  85.4 0.1 concatenate.28
  85.5 38.7 %all_gather.3 = bf16[8,32,1088]{2,0,1:T(8,128)(2,1)S(1)} all-gather(bf16[8,1,1088]{2,0,1:T(8,128)(2,1)S(1)} %concatenate.28), channel_id=1, replica_groups=mesh['dp'=4,'kv'=32,'tp'=2] {'kv'}, dimensions={1}, use_global_device_ids=true | all-gather | bytes 574464 | tf_op jit(solution)/shard_map/all_gather | solution.py:38
  124.1 0.1 split.20
  124.2 0.1 reshape.414
  124.3 0.1 broadcast_multiply_fusion
  124.3 0.1 multiply_reduce_fusion.1
  124.5 0.1 fusion.41
  124.6 0.7 fusion.58
  125.3 0.7 fusion.57
  126.0 3.3 %fusion.2 = f32[8,32,256]{2,1,0:T(8,128)S(1)} fusion(bf16[8,256,1024]{2,1,0:T(8,128)(2,1)} %param.25, pred[8,256]{1,0:T(8,128)(4,1)S(1)} %get-tuple-element.12, bf16[8,1024]{1,0:T(8,128)(2,1)S(1)} %get-tuple-element.5, bf16[8,32,1024]{2,0,1:T(8,128)(2,1)S(1)} %split.20), kind=kOutput, calls=%fused_computation.5 | convolution fusion | flops 136314880 | bytes 4999168 | tf_op jit(solution)/shard_map/shc,spc->shp/dot_general | solution.py:145
  129.2 0.0 copy-done.8
  129.2 0.3 fusion.59
  129.6 1.5 fusion.5
  131.1 0.2 fusion.23
  131.3 0.1 copy.53
  131.5 0.1 copy.52
  131.6 0.8 concatenate.30
  132.4 0.7 copy.54
  133.1 25.7 %all_to_all.29 = f32[1,8,32,1026]{3,1,0,2:T(8,128)S(1)} all-to-all(f32[1,8,32,1026]{3,1,0,2:T(8,128)S(1)} %copy.54), channel_id=1, replica_groups=mesh['dp'=4,'kv'=32,'tp'=2] {'kv'}, dimensions={2} | all-to-all | bytes 2101248 | tf_op jit(solution)/shard_map/all_to_all | solution.py:47
  158.8 3.2 %copy.55 = f32[1,8,32,1026]{2,1,3,0:T(8,128)} copy(f32[1,8,32,1026]{3,1,0,2:T(8,128)S(1)} %all_to_all.29) | data formatting | bytes 2101248 | tf_op jit(solution)/shard_map/all_to_all | solution.py:47
  162.0 0.8 slice_reduce_fusion
  162.8 0.9 fusion.48
  163.6 0.8 exponential_bitcast_fusion
  164.4 3.4 %fusion = f32[8,1024]{0,1:T(8,128)S(1)} fusion(f32[32,8,1,1026]{0,1,3,2:T(8,128)} %bitcast.75, f32[32,8]{0,1:T(8,128)S(1)} %exponential_bitcast_fusion), kind=kLoop, calls=%fused_computation.2 | loop fusion | flops 516096 | bytes 1082368 | tf_op jit(solution)/shard_map/reduce_sum | solution.py:165
  167.8 0.0 copy-done
  167.8 0.0 copy-done.9
  167.8 0.5 convolution_bitcast_fusion
  168.2 0.1 reshape.418
  168.4 0.2 copy.70
  168.5 0.2 reshape.419
  168.7 28.8 %all_to_all.30 = f32[64,1,512]{2,1,0:T(1,128)S(1)} all-to-all(f32[64,1,512]{2,1,0:T(1,128)S(1)} %reshape.419), channel_id=1, replica_groups=mesh['dp'=4,'kv'=32,'tp'=2] {'kv','tp'}, dimensions={0} | all-to-all | bytes 262144 | tf_op jit(solution)/shard_map/all_to_all | solution.py:61
  197.5 0.5 broadcast.231
  198.0 0.9 reduce.5
  199.0 0.1 reshape.420
  199.1 0.7 bitcast_reduce_fusion
  (21 shorter events, 0.1 us)
Async XLA Ops:
  0.6 167.1 %copy-start = (bf16[128,4096]{1,0:T(8,128)(2,1)S(1)}, bf16[128,4096]{1,0:T(8,128)(2,1)}, u32[]{:S(2)}) copy-start(bf16[128,4096]{1,0:T(8,128)(2,1)} %param.24) | copy-start | bytes 3145732
  4.0 15.3 %copy-start.4 = (f32[1536]{0:T(1024)S(1)}, f32[1536]{0:T(1024)}, u32[]{:S(2)}) copy-start(f32[1536]{0:T(1024)} %param.18) | copy-start | bytes 18436
  4.1 15.3 %copy-start.6 = (s32[8]{0:T(128)S(1)}, s32[8]{0:T(128)}, u32[]{:S(2)}) copy-start(s32[8]{0:T(128)} %param.27) | copy-start | bytes 100
  7.0 77.7 %copy-start.3 = (bf16[1536,1,64]{0,2,1:T(8,128)(2,1)S(1)}, bf16[1536,1,64]{0,2,1:T(8,128)(2,1)}, u32[]{:S(2)}) copy-start(bf16[1536,1,64]{0,2,1:T(8,128)(2,1)} %param.21) | copy-start | bytes 589828
  7.0 77.9 %copy-start.1 = (bf16[1536,1,128]{2,0,1:T(8,128)(2,1)S(1)}, bf16[1536,1,128]{2,0,1:T(8,128)(2,1)}, u32[]{:S(2)}) copy-start(bf16[1536,1,128]{2,0,1:T(8,128)(2,1)} %param.20) | copy-start | bytes 1179652
  7.0 77.9 %copy-start.2 = (bf16[1,128,1024]{2,1,0:T(8,128)(2,1)S(1)}, bf16[1,128,1024]{2,1,0:T(8,128)(2,1)}, u32[]{:S(2)}) copy-start(bf16[1,128,1024]{2,1,0:T(8,128)(2,1)} %param.22) | copy-start | bytes 786436
  7.0 73.7 %all-to-all-start = ((f32[32,1,21000]{2,1,0:T(1,128)}), f32[32,1,21000]{2,1,0:T(1,128)}, u32[]{:S(2)}, u32[]{:S(2)}) async-start(f32[32,1,21000]{2,1,0:T(1,128)} %broadcast_in_dim.55), calls=%async_computation | async-start | bytes 5406720 | tf_op jit(solution)/shard_map/all_to_all | solution.py:17
  19.3 105.3 %copy-start.5 = (f32[1024]{0:T(1024)S(1)}, f32[1024]{0:T(1024)}, u32[]{:S(2)}) copy-start(f32[1024]{0:T(1024)} %param.19) | copy-start | bytes 12292
  124.1 5.1 %copy-start.8 = (bf16[8,256,64]{1,2,0:T(8,128)(2,1)S(1)}, bf16[8,256,64]{1,2,0:T(8,128)(2,1)}, u32[]{:S(2)}) copy-start(bf16[8,256,64]{1,2,0:T(8,128)(2,1)} %param.26) | copy-start | bytes 786436
  124.3 5.3 %copy-start.7 = (bf16[8,256,1024]{2,1,0:T(8,128)(2,1)S(1)}, bf16[8,256,1024]{2,1,0:T(8,128)(2,1)}, u32[]{:S(2)}) copy-start(bf16[8,256,1024]{2,1,0:T(8,128)(2,1)} %param.25) | copy-start | bytes 12582916
  158.8 9.0 %copy-start.9 = (bf16[1,1024,128]{2,1,0:T(8,128)(2,1)S(1)}, bf16[1,1024,128]{2,1,0:T(8,128)(2,1)}, u32[]{:S(2)}) copy-start(bf16[1,1024,128]{2,1,0:T(8,128)(2,1)} %param.23) | copy-start | bytes 786436
where the time goes:
time: 200 us
  blocking collectives  93.2 us (47%)
  waiting for transfers between devices  61.2 us (31%)
  other arithmetic  14 us (7%)
  starting transfers between devices  12.3 us (6%)
  local copies, waits for them, and re-layouts  9.77 us (5%)
  matrix products  8.41 us (4%)
    all_to_all x1, waiting for transfers between devices, copy_for_each(): lax.all_to_all(jnp.broadcast_to(array[None], (devices, *array.shape)), ax...  61.2 us
    all_gather x1, blocking collectives, sent_together(): filled = lax.all_gather(both, axis, axis=dim, tiled=True)  38.7 us
    all_to_all x1, blocking collectives, sum_at_owner(): lax.all_to_all(cut_along(array, dim, devices), axis, 0, 0, tiled=True)  28.8 us
    all_to_all x1, blocking collectives, in_one_piece(): lax.all_to_all(both, axis, split_axis=split_dim, concat_axis=concat_dim,...  25.7 us
    all_to_all x1, starting transfers between devices, copy_for_each(): lax.all_to_all(jnp.broadcast_to(array[None], (devices, *array.shape)), ax...  12.3 us
  transfers between devices with their start and end apart: 1, of which 1 were waited for; matrix products, arithmetic and copies ran while one was open for 0% of the time, Pallas kernels for 0%

commit v1 on v0

v1 whole, which is shorter than its diff:
```python
import functools

import jax
import jax.numpy as jnp
from jax import lax
from jax.experimental import pallas as pl
from jax.experimental.pallas import tpu as pltpu
from jax.sharding import PartitionSpec as P

MODEL_BREADTH = 4096
EPS = 1e-06
THETA = 10000.0
RING = 4
MESH = pl.DeviceIdType.MESH
F32 = jnp.float32
BF16 = jnp.bfloat16


def across(a, b):
    return lax.dot_general(a, b, (((1,), (1,)), ((), ())), preferred_element_type=F32)


def plain(a, b):
    return jnp.dot(a, b, preferred_element_type=F32)


def kernel(
    depth,
    tokens_hbm,
    gain_hbm,
    ask_hbm,
    hid_hbm,
    ask_gain_hbm,
    hid_gain_hbm,
    unspun_hbm,
    spin_hbm,
    lock_hbm,
    payload_hbm,
    out_hbm,
    latent_hbm,
    rotary_hbm,
    frequency_hbm,
    lengths,
    attention_out,
    hidden_out,
    spun_out,
    tokens,
    gain,
    ask,
    hid,
    ask_gain,
    hid_gain,
    unspun,
    spin,
    lock,
    payload,
    w_out,
    latent,
    rotary,
    frequency,
    part_send,
    part_recv,
    mid_recv,
    full,
    queries,
    scores,
    spread,
    stat_send,
    stat_recv,
    mix_send,
    mix_recv,
    stat2_send,
    stat2_recv,
    mix2_send,
    mix2_recv,
    out_send,
    out_recv,
    out2_send,
    out2_recv,
    local_sem,
    part_sems,
    mid_sems,
    full_sems,
    qz_sems,
    qy_sems,
    stat_sems,
    mix_sems,
    stat2_sems,
    mix2_sems,
    out_sems,
    out2_sems,
):
    kv = lax.axis_index("kv")
    tp = lax.axis_index("tp")
    z, y = kv // RING, kv % RING
    span = 256

    def at(zz, yy, cc=None):
        where = {"kv": zz * RING + yy}
        if cc is not None:
            where["tp"] = cc
        return where

    def zp(d):
        return (z + d) % depth

    def zm(d):
        return (z + depth - d) % depth

    def yp(d):
        return (y + d) % RING

    def ym(d):
        return (y + RING - d) % RING

    pending = []

    def send(src, dst, sems, index, device):
        copy = pltpu.make_async_remote_copy(
            src_ref=src,
            dst_ref=dst,
            send_sem=sems.at[(0, *index)],
            recv_sem=sems.at[(1, *index)],
            device_id=device,
            device_id_type=MESH,
        )
        copy.start()
        pending.append(copy)
        return copy

    barrier = pltpu.get_barrier_semaphore()
    greeted = 0
    for d in range(1, depth):
        pl.semaphore_signal(barrier, inc=1, device_id=at(zp(d), y), device_id_type=MESH)
        greeted += 1
    for d in range(RING):
        for c in range(2):
            if d or c:
                pl.semaphore_signal(
                    barrier, inc=1, device_id=at(z, yp(d), (tp + c) % 2), device_id_type=MESH
                )
                greeted += 1

    loads = {}
    for k, (name, src, dst) in enumerate(
        (
            ("tokens", tokens_hbm, tokens),
            ("gain", gain_hbm, gain),
            ("ask", ask_hbm, ask),
            ("hid", hid_hbm, hid),
            ("ask_gain", ask_gain_hbm, ask_gain),
            ("hid_gain", hid_gain_hbm, hid_gain),
            ("frequency", frequency_hbm, frequency),
            ("unspun", unspun_hbm, unspun),
            ("spin", spin_hbm, spin),
            ("lock", lock_hbm, lock),
            ("rotary", rotary_hbm, rotary),
            ("latent", latent_hbm, latent),
            ("payload", payload_hbm, payload),
            ("w_out", out_hbm, w_out),
        )
    ):
        loads[name] = pltpu.make_async_copy(src, dst, local_sem.at[k])
        loads[name].start()

    for name in ("tokens", "gain", "ask", "hid"):
        loads[name].wait()
    wide = tokens[...].astype(F32)
    squares = jnp.sum(wide * wide, axis=1, keepdims=True)
    scaled = (wide * gain[...]).astype(BF16)
    query_part = plain(scaled, ask[...])
    latent_part = across(scaled, hid[...])
    tiles = [query_part[:, 128 * t : 128 * t + 128] for t in range(12)]
    tiles += [latent_part[:, 128 * t : 128 * t + 128] for t in range(8)]
    tiles += [
        jnp.concatenate([latent_part[:, 1024:1088], jnp.broadcast_to(squares, (8, 64))], axis=1)
    ]
    tiles += [jnp.zeros((8, 128), F32)] * 3
    for t, tile in enumerate(tiles):
        part_send[t // 3, t % 3] = tile
    part_recv[pl.ds(z, 1)] = part_send[pl.ds(z, 1)]

    pl.semaphore_wait(barrier, greeted)
    copies = [
        send(part_send.at[zp(d)], part_recv.at[z], part_sems, (d,), at(zp(d), y))
        for d in range(1, depth)
    ]

    for name in ("ask_gain", "hid_gain", "frequency"):
        loads[name].wait()
    row8 = lax.broadcasted_iota(jnp.int32, (8, 128), 0)
    length_rows = jnp.zeros((8, 128), jnp.int32)
    for s in range(8):
        length_rows = jnp.where(row8 == s, lengths[s], length_rows)
    angles = length_rows.astype(F32) * frequency[...]
    lane8 = lax.broadcasted_iota(jnp.int32, (8, 128), 1)
    cosine = jnp.cos(angles)
    sine = jnp.where(lane8 % 64 < 32, -jnp.sin(angles), jnp.sin(angles))

    def spinning(v):
        twice = jnp.concatenate([v, v], axis=1)
        return twice * cosine + pltpu.roll(twice, 32, 1) * sine

    for copy in copies:
        copy.wait_recv()
    total = part_recv[0]
    for j in range(1, depth):
        total = total + part_recv[j]
    mid_recv[pl.ds(y, 1)] = total[None]
    copies = [
        send(mid_recv.at[y], mid_recv.at[y], mid_sems, (d,), at(z, yp(d))) for d in range(1, RING)
    ]
    for copy in copies:
        copy.wait_recv()
    total = mid_recv[0]
    for j in range(1, RING):
        total = total + mid_recv[j]
    full[pl.ds(z, 1)] = total[None]
    copies = [
        send(full.at[z], full.at[z], full_sems, (d,), at(zp(d), y)) for d in range(1, depth)
    ]
    for name in ("unspun", "spin", "lock"):
        loads[name].wait()
    for copy in copies:
        copy.wait_recv()

    last = full[6, 2]
    row_scale = lax.rsqrt(last[:, 64:65] / MODEL_BREADTH + EPS)
    query_down = jnp.concatenate([full[t // 3, t % 3] for t in range(12)], axis=1) * row_scale
    mean_square = jnp.mean(query_down * query_down, axis=1, keepdims=True)
    squeezed = (query_down * lax.rsqrt(mean_square + EPS) * ask_gain[...]).astype(BF16)
    nope = plain(squeezed, unspun[...]).astype(BF16)
    turned = spinning(across(squeezed, spin[...])).astype(BF16)
    queries[0, 0, :, 1024:1152] = turned
    queries[0, 0, :, 0:1024] = plain(nope, lock[...]).astype(BF16)

    order = sorted(range(1, depth), key=lambda d: min(d, depth - d))
    from_z = {
        d: send(queries.at[0, 0], queries.at[0, d], qz_sems, (d,), at(zp(d), y)) for d in order
    }
    from_y = [
        send(queries.at[0, 0], queries.at[e, 0], qy_sems, (e, 0), at(z, yp(e)))
        for e in range(1, RING)
    ]

    hidden_down = jnp.concatenate([full[t // 3, t % 3] for t in range(12, 20)], axis=1) * row_scale
    mean_square = jnp.mean(hidden_down * hidden_down, axis=1, keepdims=True)
    incoming_hidden = hidden_down * lax.rsqrt(mean_square + EPS) * hid_gain[...]
    incoming_spun = spinning(last[:, 0:64] * row_scale)[:, 0:64]
    hidden_out[...] = incoming_hidden
    spun_out[...] = incoming_spun

    def forward(d):
        from_z[d].wait_recv()
        for e in range(1, RING):
            from_y.append(
                send(queries.at[0, d], queries.at[e, d], qy_sems, (e, d), at(z, yp(e)))
            )

    loads["latent"].wait()
    loads["rotary"].wait()
    eye = (
        lax.broadcasted_iota(jnp.int32, (64, 64), 0) == lax.broadcasted_iota(jnp.int32, (64, 64), 1)
    ).astype(BF16)
    spun_columns = across(eye, incoming_spun.astype(BF16))
    position_row = kv * span + lax.broadcasted_iota(jnp.int32, (64, span), 1)
    position_column = kv * span + lax.broadcasted_iota(jnp.int32, (span, 1024), 0)
    for s in range(8):
        rotary[s] = jnp.where(
            position_row == lengths[s], spun_columns[:, s : s + 1], rotary[s].astype(F32)
        ).astype(BF16)
        latent[span * s : span * s + span] = jnp.where(
            position_column == lengths[s],
            incoming_hidden[s : s + 1],
            latent[span * s : span * s + span].astype(F32),
        ).astype(BF16)
        if s < depth - 1:
            forward(order[s])
    for copy in from_y:
        copy.wait_recv()

    rows = 8 * RING * depth
    everything = queries[...].reshape(rows, 1152)
    sequence = lax.broadcasted_iota(jnp.int32, (rows, span), 0) % 8

    @pl.loop(0, 8)
    def _(s):
        block = latent[pl.ds(pl.multiple_of(s * span, span), span), :]
        found = across(everything[:, 0:1024], block) + plain(everything[:, 1024:1088], rotary[s])
        scores[...] = jnp.where(sequence == s, found, scores[...])

    grouped = (RING * depth, 8, span)
    position = kv * span + lax.broadcasted_iota(jnp.int32, grouped, 2)
    lengths_wide = jnp.concatenate([length_rows, length_rows], axis=1)
    visible = position <= lengths_wide[None]
    score = jnp.where(visible, scores[...].reshape(grouped) * (192.0**-0.5), -1e30)
    highest = jnp.max(score, axis=2, keepdims=True)
    high = highest.astype(BF16).astype(F32)
    low = (highest - high).astype(BF16).astype(F32)
    highest = high + low
    weight = jnp.where(visible, jnp.exp(score - highest), 0.0)
    denominator = jnp.sum(weight, axis=2, keepdims=True)

    def statistics(m_high, m_low, total):
        t_high = total.astype(BF16).astype(F32)
        lane = lax.broadcasted_iota(jnp.int32, (*total.shape[:2], 128), 2)
        return jnp.where(
            lane == 0,
            m_high,
            jnp.where(lane == 1, m_low, jnp.where(lane == 2, t_high, total - t_high)),
        ).astype(BF16)

    stat_send[...] = statistics(high, low, denominator).reshape(RING, depth, 8, 128)
    stat_copies = [
        send(stat_send.at[e], stat_recv.at[e], stat_sems, (e,), at(z, ym(e)))
        for e in range(1, RING)
    ]
    flat = weight.reshape(rows, span)
    for s in range(8):
        spread[:, span * s : span * s + span] = jnp.where(sequence == s, flat, 0.0).astype(BF16)

    mix_copies = []
    for n in range(4):
        found = plain(spread[...], latent[:, 256 * n : 256 * n + 256])
        mix_send[n] = found.astype(BF16).reshape(RING, depth, 8, 256)
        mix_copies.append(
            [
                send(mix_send.at[n, e], mix_recv.at[n, e], mix_sems, (n, e), at(z, ym(e)))
                for e in range(1, RING)
            ]
        )

    def combine(stats):
        tops = [b[:, :, 0:1] + b[:, :, 1:2] for b in stats]
        sums = [b[:, :, 2:3] + b[:, :, 3:4] for b in stats]
        top = functools.reduce(jnp.maximum, tops)
        factors = [jnp.exp(t - top) for t in tops]
        return top, sum(f * v for f, v in zip(factors, sums)), factors

    for copy in stat_copies:
        copy.wait_recv()
    top, total, factors = combine(
        [stat_send[0].astype(F32)] + [stat_recv[e].astype(F32) for e in range(1, RING)]
    )
    high = top.astype(BF16).astype(F32)
    stat2_send[...] = statistics(high, top - high, total)
    stat2_copies = [
        send(stat2_send.at[d], stat2_recv.at[d], stat2_sems, (d,), at(zm(d), y))
        for d in range(1, depth)
    ]
    mix2_copies = []
    for n in range(4):
        for copy in mix_copies[n]:
            copy.wait_recv()
        found = factors[0] * mix_send[n, 0].astype(F32)
        for e in range(1, RING):
            found = found + factors[e] * mix_recv[n, e].astype(F32)
        mix2_send[n] = found.astype(BF16)
        mix2_copies.append(
            [
                send(mix2_send.at[n, d], mix2_recv.at[n, d], mix2_sems, (n, d), at(zm(d), y))
                for d in range(1, depth)
            ]
        )

    for copy in stat2_copies:
        copy.wait_recv()
    _, total, factors = combine(
        [stat2_send[0:1].astype(F32)] + [stat2_recv[d : d + 1].astype(F32) for d in range(1, depth)]
    )
    factors = [f[0] for f in factors]
    attended = []
    for n in range(4):
        for copy in mix2_copies[n]:
            copy.wait_recv()
        found = factors[0] * mix2_send[n, 0].astype(F32)
        for d in range(1, depth):
            found = found + factors[d] * mix2_recv[n, d].astype(F32)
        attended.append((found / total[0]).astype(BF16))

    loads["payload"].wait()
    loads["w_out"].wait()
    values = plain(jnp.concatenate(attended, axis=1), payload[...]).astype(BF16)
    projected = plain(values, w_out[...])
    first = lane8 < 64
    for i in range(depth // 2):
        for j in range(RING):
            a = 128 * (2 * i * RING + j)
            b = 128 * ((2 * i + 1) * RING + j)
            one, two = projected[:, a : a + 128], projected[:, b : b + 128]
            out_send[j, 0, i] = jnp.where(first, one, pltpu.roll(two, 64, 1)).astype(BF16)
            out_send[j, 1, i] = jnp.where(first, pltpu.roll(one, 64, 1), two).astype(BF16)
    copies = []
    for e in range(RING):
        for c in range(2):
            if e or c:
                core = (tp + c) % 2
                copies.append(
                    send(
                        out_send.at[yp(e), core],
                        out_recv.at[2 * e + c],
                        out_sems,
                        (2 * e + c,),
                        at(z, yp(e), core),
                    )
                )
    found = out_send[y, tp].astype(F32)
    for copy in copies:
        copy.wait_recv()
    for k in range(1, 2 * RING):
        found = found + out_recv[k].astype(F32)
    out2_send[...] = found.astype(BF16)
    copies = [
        send(out2_send.at[zp(d) // 2], out2_recv.at[d], out2_sems, (d,), at(zp(d), y))
        for d in range(1, depth)
    ]
    found = out2_send[z // 2].astype(F32)
    for copy in copies:
        copy.wait_recv()
    for d in range(1, depth):
        found = found + out2_recv[d].astype(F32)
    attention_out[...] = jnp.where(z % 2 == 0, found[:, 0:64], found[:, 64:128])
    for copy in pending:
        copy.wait_send()


def local(
    depth,
    tokens,
    token_gain,
    asker_narrow_matrix,
    hidden_narrow_matrix,
    asker_multiplier,
    hidden_multiplier,
    asker_unspun_matrix,
    asker_spin_matrix,
    lock_widen_matrix,
    payload_widen_matrix,
    w_output,
    cache_latent,
    cache_rotary,
    lengths,
):
    exponent = (jnp.arange(128) % 32).astype(F32) * (2.0 / 64)
    frequency = (THETA ** (-exponent))[None]
    operands = (
        tokens,
        token_gain.reshape(1, 128),
        asker_narrow_matrix,
        hidden_narrow_matrix.T,
        asker_multiplier.reshape(1, 1536),
        hidden_multiplier.reshape(1, 1024),
        asker_unspun_matrix.reshape(1536, 128),
        asker_spin_matrix.reshape(1536, 64).T,
        lock_widen_matrix.reshape(128, 1024),
        payload_widen_matrix.reshape(1024, 128),
        w_output,
        cache_latent.reshape(2048, 1024),
        jnp.swapaxes(cache_rotary, 1, 2),
        frequency,
    )
    hbm = pl.BlockSpec(memory_space=pl.ANY)
    vmem = pl.BlockSpec(memory_space=pltpu.VMEM)
    dma = pltpu.SemaphoreType.DMA
    return pl.pallas_call(
        functools.partial(kernel, depth),
        out_shape=(
            jax.ShapeDtypeStruct((8, 64), F32),
            jax.ShapeDtypeStruct((8, 1024), F32),
            jax.ShapeDtypeStruct((8, 64), F32),
        ),
        in_specs=[hbm] * len(operands) + [pl.BlockSpec(memory_space=pltpu.SMEM)],
        out_specs=(vmem, vmem, vmem),
        scratch_shapes=[pltpu.VMEM(a.shape, a.dtype) for a in operands]
        + [
            pltpu.VMEM((depth, 3, 8, 128), F32),
            pltpu.VMEM((depth, 3, 8, 128), F32),
            pltpu.VMEM((RING, 3, 8, 128), F32),
            pltpu.VMEM((depth, 3, 8, 128), F32),
            pltpu.VMEM((RING, depth, 8, 1152), BF16),
            pltpu.VMEM((8 * RING * depth, 256), F32),
            pltpu.VMEM((8 * RING * depth, 2048), BF16),
            pltpu.VMEM((RING, depth, 8, 128), BF16),
            pltpu.VMEM((RING, depth, 8, 128), BF16),
            pltpu.VMEM((4, RING, depth, 8, 256), BF16),
            pltpu.VMEM((4, RING, depth, 8, 256), BF16),
            pltpu.VMEM((depth, 8, 128), BF16),
            pltpu.VMEM((depth, 8, 128), BF16),
            pltpu.VMEM((4, depth, 8, 256), BF16),
            pltpu.VMEM((4, depth, 8, 256), BF16),
            pltpu.VMEM((RING, 2, depth // 2, 8, 128), BF16),
            pltpu.VMEM((2 * RING, depth // 2, 8, 128), BF16),
            pltpu.VMEM((depth // 2, 8, 128), BF16),
            pltpu.VMEM((depth, 8, 128), BF16),
            dma((len(operands),)),
            dma((2, depth)),
            dma((2, RING)),
            dma((2, depth)),
            dma((2, depth)),
            dma((2, RING, depth)),
            dma((2, RING)),
            dma((2, 4, RING)),
            dma((2, depth)),
            dma((2, 4, depth)),
            dma((2, 2 * RING)),
            dma((2, depth)),
        ],
        compiler_params=pltpu.CompilerParams(collective_id=0, has_side_effects=True),
    )(*operands, lengths)


def solution(mesh):
    return jax.shard_map(
        functools.partial(local, mesh.shape["kv"] // RING),
        mesh=mesh,
        in_specs=(
            P("dp", "kv"),
            P("kv"),
            P("kv", None),
            P("kv", None),
            P(),
            P(),
            P(None, ("kv", "tp"), None),
            P(None, ("kv", "tp"), None),
            P(("kv", "tp"), None, None),
            P(("kv", "tp"), None, None),
            P(("kv", "tp"), None),
            P("dp", "kv", None),
            P("dp", "kv", None),
            P("dp"),
        ),
        out_specs=(P("dp", ("kv", "tp")), P("dp", None), P("dp", None)),
        check_vma=False,
    )
```

time: 200 us -> 65.8 us (0.33)
  blocking collectives: 93.2 us -> 0 us
  waiting for transfers between devices: 61.2 us -> 0 us
  Pallas kernels: 0 us -> 59.1 us
  other arithmetic: 14 us -> 0.52 us
  starting transfers between devices: 12.3 us -> 0 us
  matrix products: 8.41 us -> 0 us
  local copies, waits for them, and re-layouts: 9.77 us -> 5.21 us
    all_to_all x1 -> x0, waiting for transfers between devices: 61.2 us -> none  [copy_for_each(): lax.all_to_all(jnp.broadcast_to(array[None], (devices, *array.shape)), ax...]
    pallas_call x0 -> x1, Pallas kernels: none -> 59.1 us  [local(): pl.pallas_call(functools.partial(kernel, depth), out_shape=(jax.ShapeDtyp...]
    all_to_all x2 -> x0, blocking collectives: 54.5 us -> none  [the longest x1 28.8 us: sum_at_owner(): lax.all_to_all(cut_along(array, dim, devices), axis, 0, 0, tiled=True)]
    all_gather x1 -> x0, blocking collectives: 38.7 us -> none  [sent_together(): filled = lax.all_gather(both, axis, axis=dim, tiled=True)]
    all_to_all x1 -> x0, starting transfers between devices: 12.3 us -> none  [copy_for_each(): lax.all_to_all(jnp.broadcast_to(array[None], (devices, *array.shape)), ax...]
    reduce_sum x8 -> x0, other arithmetic: 9.61 us -> none  [the longest x1 3.38 us: local(): mixture = jnp.sum(taken_mix * factor[..., None], axis=0)]
    dot_general x8 -> x0, matrix products: 8.41 us -> none  [the longest x1 3.28 us: local(): jnp.einsum('shc,spc->shp', all_latent, keys_latent, preferred_element_typ...]
    all_to_all x2 -> x0, local copies, waits for them, and re-layouts: 3.68 us -> none  [the longest x1 3.17 us: in_one_piece(): lax.all_to_all(both, axis, split_axis=split_dim, concat_axis=concat_dim,...]
  transfers between devices with their start and end apart: 1 -> 0, of which waited for: 1 -> 0; matrix products, arithmetic and copies ran while one was open for 0% -> 0% of each run, Pallas kernels for 0% -> 0%
where the time goes in v1:
time: 65.8 us; the launch traced here: 65.5 us
  Pallas kernels  59.1 us (90%)
  local copies, waits for them, and re-layouts  5.21 us (8%)
    pallas_call x1, Pallas kernels, local(): pl.pallas_call(functools.partial(kernel, depth), out_shape=(jax.ShapeDtyp...  59.1 us
    unnamed x3, local copies, waits for them, and re-layouts  3.91 us

profile of v1, /device:TPU:1, one launch (start us, length us, event | category | flops | bytes accessed | tf_op | source)
XLA Modules:
  0.0 65.5 jit_solution(14681464808454174055)
XLA Ops:
  0.6 0.5 fusion.3.frequency_hbm
  1.2 1.3 %reshape.65.ask_gain_hbm = f32[1,1536]{1,0:T(1,128)} reshape(f32[1536]{0:T(1024)} %param.18) | data formatting | bytes 12288 | tf_op jit(solution)/shard_map/reshape | solution.py:451
  2.4 59.1 %shard_map.157 = (f32[8,64]{1,0:T(8,128)}, f32[8,1024]{1,0:T(8,128)}, f32[8,64]{1,0:T(8,128)}) custom-call(bf16[8,128]{1,0:T(8,128)(2,1)} %tokens_hbm.1, f32[1,128]{1,0:T(1,128)} %bitcast.19, bf16[128,1536]{1,0:T(8,128)(2,1)} %ask_hbm.1, bf16[1088,128]{1,0:T(8,128)(2,1)} %bitcast.13, f32[1,1536]{1,0:T(1,128)} %reshape.65.ask_gain_hbm, f32[1,1024]{1,0:T(1,128)} %bitcast.18, ...), custom_call_target="tpu_custom_call" | custom-call | tf_op jit(solution)/shard_map/pallas_call | solution.py:465
  61.6 1.3 %copy.20 = f32[8,64]{1,0:T(8,128)} copy(f32[8,64]{1,0:T(8,128)} %get-tuple-element.6) | data formatting | bytes 4096
  62.9 1.4 %copy.21 = f32[8,1024]{1,0:T(8,128)} copy(f32[8,1024]{1,0:T(8,128)} %get-tuple-element.7) | data formatting | bytes 65536
  64.2 1.3 %copy.22 = f32[8,64]{1,0:T(8,128)} copy(f32[8,64]{1,0:T(8,128)} %get-tuple-element.8) | data formatting | bytes 4096

commit v2 on v1

v2 whole, which is shorter than its diff:
```python
import functools

import jax
import jax.numpy as jnp
from jax import lax
from jax.experimental import pallas as pl
from jax.experimental.pallas import tpu as pltpu
from jax.sharding import PartitionSpec as P

MODEL_BREADTH = 4096
EPS = 1e-06
THETA = 10000.0
RING = 4
MESH = pl.DeviceIdType.MESH
PART, MID, FULL, ASK_Y, ASK_Z, MIX, MIX2, OUT, OUT2, PHASES = 0, 1, 2, 3, 8, 16, 24, 25, 26, 27
F32 = jnp.float32
BF16 = jnp.bfloat16


def across(a, b):
    return lax.dot_general(a, b, (((1,), (1,)), ((), ())), preferred_element_type=F32)


def plain(a, b):
    return jnp.dot(a, b, preferred_element_type=F32)


def kernel(
    depth,
    tokens_hbm,
    gain_hbm,
    ask_hbm,
    hid_hbm,
    ask_gain_hbm,
    hid_gain_hbm,
    unspun_hbm,
    spin_hbm,
    lock_hbm,
    payload_hbm,
    out_hbm,
    latent_hbm,
    rotary_hbm,
    lengths_hbm,
    attention_out,
    hidden_out,
    spun_out,
    tokens,
    gain,
    ask,
    hid,
    ask_gain,
    hid_gain,
    unspun,
    spin,
    lock,
    payload,
    w_out,
    latent,
    rotary,
    part_send,
    part_recv,
    mid_recv,
    full,
    queries,
    sorted_queries,
    mix_own,
    mix_send,
    mix_recv,
    mix2_send,
    mix2_recv,
    out_send,
    out_recv,
    out2_send,
    out2_recv,
    local_sem,
    sent_sems,
    come_sems,
    lengths,
):
    kv = lax.axis_index("kv")
    tp = lax.axis_index("tp")
    z, y = kv // RING, kv % RING
    span = 256
    near_first = sorted(range(1, depth), key=lambda d: min(d, depth - d))
    order = (1, 3, 2)

    def at(zz, yy, cc=None):
        where = {"kv": zz * RING + yy}
        if cc is not None:
            where["tp"] = cc
        return where

    def zp(d):
        return (z + d) % depth

    def zm(d):
        return (z + depth - d) % depth

    def yp(d):
        return (y + d) % RING

    def ym(d):
        return (y + RING - d) % RING

    def describe(src, dst, phase, arrival, device):
        return pltpu.make_async_remote_copy(
            src_ref=src,
            dst_ref=dst,
            send_sem=sent_sems.at[phase],
            recv_sem=come_sems.at[arrival],
            device_id=device,
            device_id_type=MESH,
        )

    def send(src, dst, phase, arrival, device):
        describe(src, dst, phase, arrival, device).start()

    def arrived(ref, arrival):
        describe(ref, ref, 0, arrival, at(z, y)).wait_recv()

    plane = [(e, c) for e in (*order, 0) for c in range(2) if e or c]

    barrier = pltpu.get_barrier_semaphore()
    for d in near_first:
        pl.semaphore_signal(barrier, inc=1, device_id=at(zp(d), y), device_id_type=MESH)
    for e, c in plane:
        pl.semaphore_signal(
            barrier, inc=1, device_id=at(z, yp(e), (tp + c) % 2), device_id_type=MESH
        )
    greeted = len(near_first) + len(plane)

    loads = {}

    def load(**pairs):
        for name, (src, dst) in pairs.items():
            loads[name] = pltpu.make_async_copy(src, dst, local_sem.at[len(started)])
            started.append(name)
            loads[name].start()

    started = []
    load(
        tokens=(tokens_hbm, tokens),
        gain=(gain_hbm, gain),
        ask=(ask_hbm, ask),
        hid=(hid_hbm, hid),
    )

    for name in ("tokens", "gain", "ask", "hid"):
        loads.pop(name).wait()
    load(
        lengths=(lengths_hbm, lengths),
        ask_gain=(ask_gain_hbm, ask_gain),
        hid_gain=(hid_gain_hbm, hid_gain),
        unspun=(unspun_hbm, unspun),
        spin=(spin_hbm, spin),
        lock=(lock_hbm, lock),
        rotary=(rotary_hbm, rotary),
        latent=(latent_hbm, latent),
        payload=(payload_hbm, payload),
        w_out=(out_hbm, w_out),
    )
    wide = tokens[...].astype(F32)
    squares = jnp.sum(wide * wide, axis=1, keepdims=True)
    scaled = (wide * gain[...]).astype(BF16)
    query_part = plain(scaled, ask[...])
    latent_part = across(scaled, hid[...])
    tiles = [query_part[:, 128 * t : 128 * t + 128] for t in range(12)]
    tiles += [latent_part[:, 128 * t : 128 * t + 128] for t in range(8)]
    tiles += [
        jnp.concatenate([latent_part[:, 1024:1088], jnp.broadcast_to(squares, (8, 64))], axis=1)
    ]
    tiles += [jnp.zeros((8, 128), F32)] * 3
    for t, tile in enumerate(tiles):
        part_send[t // 6, t // 3 % 2, t % 3] = tile

    pl.semaphore_wait(barrier, greeted)
    for e in order:
        send(part_send.at[yp(e), tp], part_recv.at[e - 1], PART, PART, at(z, yp(e)))

    loads.pop("lengths").wait()
    row8 = lax.broadcasted_iota(jnp.int32, (8, 128), 0)
    lane8 = lax.broadcasted_iota(jnp.int32, (8, 128), 1)
    length_rows = jnp.zeros((8, 128), jnp.int32)
    frequency = jnp.zeros((8, 128), F32)
    for s in range(8):
        length_rows = jnp.where(row8 == s, lengths[s], length_rows)
    for i in range(32):
        frequency = jnp.where(lane8 % 32 == i, float(THETA ** (-i / 32)), frequency)
    angles = length_rows.astype(F32) * frequency
    cosine = jnp.cos(angles)
    sine = jnp.where(lane8 % 64 < 32, -jnp.sin(angles), jnp.sin(angles))

    def spinning(v):
        twice = jnp.concatenate([v, v], axis=1)
        return twice * cosine + pltpu.roll(twice, 32, 1) * sine

    total = part_send[y, tp]
    arrived(part_recv, PART)
    for e in range(RING - 1):
        total = total + part_recv[e]
    mid_recv[pl.ds(z, 1)] = total[None]
    for d in near_first:
        send(mid_recv.at[z], mid_recv.at[z], MID, MID, at(zp(d), y))
    arrived(mid_recv.at[1:depth], MID)
    total = mid_recv[0]
    for j in range(1, depth):
        total = total + mid_recv[j]
    full[pl.ds(2 * y + tp, 1)] = total[None]
    mine = full.at[2 * y + tp]
    for e, c in plane:
        send(mine, mine, FULL, FULL, at(z, yp(e), (tp + c) % 2))
    for name in ("unspun", "spin", "lock", "ask_gain", "hid_gain"):
        loads.pop(name).wait()
    arrived(full.at[1 : 2 * RING], FULL)

    last = full[6, 2]
    row_scale = lax.rsqrt(last[:, 64:65] / MODEL_BREADTH + EPS)
    query_down = jnp.concatenate([full[t // 3, t % 3] for t in range(12)], axis=1) * row_scale
    mean_square = jnp.mean(query_down * query_down, axis=1, keepdims=True)
    ask_gains = jnp.concatenate([ask_gain[t : t + 1] for t in range(12)], axis=1)
    squeezed = (query_down * lax.rsqrt(mean_square + EPS) * ask_gains).astype(BF16)
    nope = plain(squeezed, unspun[...]).astype(BF16)
    turned = spinning(across(squeezed, spin[...])).astype(BF16)
    queries[0, 0, :, 1024:1152] = turned
    queries[0, 0, :, 0:1024] = plain(nope, lock[...]).astype(BF16)

    def to_plane(d):
        for e in order:
            send(queries.at[0, d], queries.at[e, d], ASK_Y, ASK_Y + e, at(z, yp(e)))

    for d in near_first:
        send(queries.at[0, 0], queries.at[0, d], ASK_Z, ASK_Z + d, at(zp(d), y))
    to_plane(0)

    hidden_down = jnp.concatenate([full[t // 3, t % 3] for t in range(12, 20)], axis=1) * row_scale
    mean_square = jnp.mean(hidden_down * hidden_down, axis=1, keepdims=True)
    incoming_hidden = hidden_down * lax.rsqrt(mean_square + EPS) * hid_gain[...]
    incoming_spun = spinning(last[:, 0:64] * row_scale)[:, 0:64]
    hidden_out[...] = incoming_hidden
    spun_out[...] = incoming_spun

    loads.pop("latent").wait()
    loads.pop("rotary").wait()
    eye = (
        lax.broadcasted_iota(jnp.int32, (64, 64), 0) == lax.broadcasted_iota(jnp.int32, (64, 64), 1)
    ).astype(BF16)
    spun_columns = across(eye, incoming_spun.astype(BF16))
    position_row = kv * span + lax.broadcasted_iota(jnp.int32, (64, span), 1)
    position_column = kv * span + lax.broadcasted_iota(jnp.int32, (span, 1024), 0)
    for s in range(8):
        rotary[s] = jnp.where(
            position_row == lengths[s], spun_columns[:, s : s + 1], rotary[s].astype(F32)
        ).astype(BF16)
        latent[span * s : span * s + span] = jnp.where(
            position_column == lengths[s],
            incoming_hidden[s : s + 1],
            latent[span * s : span * s + span].astype(F32),
        ).astype(BF16)
        if s < depth - 1:
            d = near_first[s]
            arrived(queries.at[0, d], ASK_Z + d)
            to_plane(d)

    group = 8 * depth
    come = lax.broadcasted_iota(jnp.int32, (group, group), 1)
    went = lax.broadcasted_iota(jnp.int32, (group, group), 0)
    shuffle = (come == went % depth * 8 + went // depth).astype(BF16)

    def sort_rows(e):
        found = plain(shuffle, queries[e].reshape(group, 1152)).astype(BF16)
        sorted_queries[:, e] = found.reshape(8, depth, 1152)

    sort_rows(0)
    for e in order:
        arrived(queries.at[e], ASK_Y + e)
        sort_rows(e)

    heads = RING * depth
    position = kv * span + lax.broadcasted_iota(jnp.int32, (heads, span), 1)
    lane = lax.broadcasted_iota(jnp.int32, (heads, 128), 1)

    def halves(value):
        high = value.astype(BF16).astype(F32)
        return high, (value - high).astype(BF16).astype(F32)

    def score(s):
        block = latent[span * s : span * s + span]
        asked = sorted_queries[s].reshape(heads, 1152)
        return across(asked[:, 0:1024], block) + plain(asked[:, 1024:1088], rotary[s])

    def soften(s, found):
        visible = position <= lengths[s]
        found = jnp.where(visible, found * (192.0**-0.5), -1e30)
        high, low = halves(jnp.max(found, axis=1, keepdims=True))
        weight = jnp.where(visible, jnp.exp(found - (high + low)), 0.0)
        t_high, t_low = halves(jnp.sum(weight, axis=1, keepdims=True))
        stats = jnp.where(
            lane == 0,
            high,
            jnp.where(lane == 1, low, jnp.where(lane == 2, t_high, t_low)),
        )
        return weight.astype(BF16), stats

    def mix(s, weight, stats):
        found = plain(weight, latent[span * s : span * s + span])
        mix_own[s, :, 0:1024] = found[0:depth]
        mix_own[s, :, 1024:1152] = stats[0:depth]
        mix_send[s, :, :, 0:1024] = found[depth:].astype(BF16).reshape(RING - 1, depth, 1024)
        mix_send[s, :, :, 1024:1152] = stats[depth:].astype(BF16).reshape(RING - 1, depth, 128)
        for e in order:
            send(mix_send.at[s, e - 1], mix_recv.at[s, e - 1], MIX, MIX + s, at(z, ym(e)))

    found = {0: score(0)}
    for s in range(8):
        if s < 7:
            found[s + 1] = score(s + 1)
        mix(s, *soften(s, found.pop(s)))

    def combine(parts):
        tops = [p[:, 1024:1025] + p[:, 1025:1026] for p in parts]
        sums = [p[:, 1026:1027] + p[:, 1027:1028] for p in parts]
        top = functools.reduce(jnp.maximum, tops)
        factors = [jnp.exp(t - top) for t in tops]
        total = sum(f * v for f, v in zip(factors, sums))
        return top, total, sum(f * p[:, 0:1024] for f, p in zip(factors, parts))

    lane8k = lane[0:depth]
    for s in range(8):
        arrived(mix_recv.at[s], MIX + s)
        top, total, found = combine(
            [mix_own[s]] + [mix_recv[s, e].astype(F32) for e in range(RING - 1)]
        )
        mix2_send[s, :, 0:1024] = found
        mix2_send[s, :, 1024:1152] = jnp.where(
            lane8k == 0, top, jnp.where(lane8k == 2, total, 0.0)
        )
        for d in near_first:
            own, theirs = mix2_send.at[s, pl.ds(d, 1)], mix2_recv.at[d, pl.ds(s, 1)]
            send(own, theirs, MIX2, MIX2, at(zm(d), y))
        mix2_recv[0, s : s + 1] = mix2_send[s, 0:1]

    loads.pop("payload").wait()
    loads.pop("w_out").wait()
    arrived(mix2_recv.at[1:depth], MIX2)
    _, total, found = combine([mix2_recv[d] for d in range(depth)])
    attended = (found / total).astype(BF16)

    values = plain(attended, payload[...]).astype(BF16)
    projected = plain(values, w_out[...])
    first = lane8 < 64
    for i in range(depth // 2):
        for j in range(RING):
            a = 128 * (2 * i * RING + j)
            b = 128 * ((2 * i + 1) * RING + j)
            one, two = projected[:, a : a + 128], projected[:, b : b + 128]
            out_send[j, 0, i] = jnp.where(first, one, pltpu.roll(two, 64, 1)).astype(BF16)
            out_send[j, 1, i] = jnp.where(first, pltpu.roll(one, 64, 1), two).astype(BF16)
    for e, c in plane:
        core = (tp + c) % 2
        theirs = out_recv.at[2 * e + c]
        send(out_send.at[yp(e), core], theirs, OUT, OUT, at(z, yp(e), core))
    found = out_send[y, tp].astype(F32)
    arrived(out_recv.at[1 : 2 * RING], OUT)
    for k in range(1, 2 * RING):
        found = found + out_recv[k].astype(F32)
    out2_send[...] = found.astype(BF16)
    for d in near_first:
        send(out2_send.at[zp(d) // 2], out2_recv.at[d], OUT2, OUT2, at(zp(d), y))
    found = out2_send[z // 2].astype(F32)
    arrived(out2_recv.at[1:depth], OUT2)
    for d in range(1, depth):
        found = found + out2_recv[d].astype(F32)
    attention_out[...] = jnp.where(z % 2 == 0, found[:, 0:64], found[:, 64:128])

    for ref, phase in (
        (part_recv, PART),
        (mid_recv.at[1:depth], MID),
        (full.at[1 : 2 * RING], FULL),
        (queries.at[0, 1:depth], ASK_Z),
        (queries.at[1:RING], ASK_Y),
        (mix_send, MIX),
        (mix2_recv.at[1:depth], MIX2),
        (out_recv.at[1 : 2 * RING], OUT),
        (out2_recv.at[1:depth], OUT2),
    ):
        describe(ref, ref, phase, 0, at(z, y)).wait_send()


def settle(a, b, c, to_a, to_b, to_c):
    to_a[...] = a[...]
    to_b[...] = b[...]
    to_c[...] = c[...]


def local(
    depth,
    tokens,
    token_gain,
    asker_narrow_matrix,
    hidden_narrow_matrix,
    asker_multiplier,
    hidden_multiplier,
    asker_unspun_matrix,
    asker_spin_matrix,
    lock_widen_matrix,
    payload_widen_matrix,
    w_output,
    cache_latent,
    cache_rotary,
    lengths,
):
    operands = (
        tokens,
        token_gain.reshape(1, 128),
        asker_narrow_matrix,
        hidden_narrow_matrix.T,
        asker_multiplier.reshape(12, 128),
        hidden_multiplier.reshape(1, 1024),
        asker_unspun_matrix.reshape(1536, 128),
        asker_spin_matrix.reshape(1536, 64).T,
        lock_widen_matrix.reshape(128, 1024),
        payload_widen_matrix.reshape(1024, 128),
        w_output,
        cache_latent.reshape(2048, 1024),
        jnp.swapaxes(cache_rotary, 1, 2),
    )
    hbm = pl.BlockSpec(memory_space=pl.ANY)
    vmem = pl.BlockSpec(memory_space=pltpu.VMEM)
    dma = pltpu.SemaphoreType.DMA
    shapes = tuple(jax.ShapeDtypeStruct((8, w), F32) for w in (64, 1024, 64))
    found = pl.pallas_call(
        functools.partial(kernel, depth),
        out_shape=shapes,
        in_specs=[hbm] * (len(operands) + 1),
        out_specs=(vmem, vmem, vmem),
        scratch_shapes=[pltpu.VMEM(a.shape, a.dtype) for a in operands]
        + [
            pltpu.VMEM((RING, 2, 3, 8, 128), F32),
            pltpu.VMEM((RING - 1, 3, 8, 128), F32),
            pltpu.VMEM((depth, 3, 8, 128), F32),
            pltpu.VMEM((2 * RING, 3, 8, 128), F32),
            pltpu.VMEM((RING, depth, 8, 1152), BF16),
            pltpu.VMEM((8, RING, depth, 1152), BF16),
            pltpu.VMEM((8, depth, 1152), F32),
            pltpu.VMEM((8, RING - 1, depth, 1152), BF16),
            pltpu.VMEM((8, RING - 1, depth, 1152), BF16),
            pltpu.VMEM((8, depth, 1152), F32),
            pltpu.VMEM((depth, 8, 1152), F32),
            pltpu.VMEM((RING, 2, depth // 2, 8, 128), BF16),
            pltpu.VMEM((2 * RING, depth // 2, 8, 128), BF16),
            pltpu.VMEM((depth // 2, 8, 128), BF16),
            pltpu.VMEM((depth, 8, 128), BF16),
            dma((len(operands) + 1,)),
            dma((PHASES,)),
            dma((PHASES,)),
            pltpu.SMEM((8,), jnp.int32),
        ],
        compiler_params=pltpu.CompilerParams(collective_id=0, has_side_effects=True),
    )(*operands, lengths)
    return pl.pallas_call(
        settle, out_shape=shapes, in_specs=[vmem] * 3, out_specs=(vmem, vmem, vmem)
    )(*found)


def solution(mesh):
    return jax.shard_map(
        functools.partial(local, mesh.shape["kv"] // RING),
        mesh=mesh,
        in_specs=(
            P("dp", "kv"),
            P("kv"),
            P("kv", None),
            P("kv", None),
            P(),
            P(),
            P(None, ("kv", "tp"), None),
            P(None, ("kv", "tp"), None),
            P(("kv", "tp"), None, None),
            P(("kv", "tp"), None, None),
            P(("kv", "tp"), None),
            P("dp", "kv", None),
            P("dp", "kv", None),
            P("dp"),
        ),
        out_specs=(P("dp", ("kv", "tp")), P("dp", None), P("dp", None)),
        check_vma=False,
    )
```

time: 65.8 us -> 59.7 us (0.907)
  local copies, waits for them, and re-layouts: 5.21 us -> 0 us
    unnamed x3 -> x0, local copies, waits for them, and re-layouts: 3.91 us -> none
    reshape x1 -> x0, local copies, waits for them, and re-layouts: 1.29 us -> none  [local(): asker_multiplier.reshape(1, 1536)]
    pallas_call x1 -> x2, Pallas kernels: 59.1 us -> 58.9 us  [the longest x1 57.5 us: local(): pl.pallas_call(functools.partial(kernel, depth), out_shape=shapes, in_spe...]
where the time goes in v2:
time: 59.7 us; the launch traced here: 59.5 us
  Pallas kernels  58.9 us (99%)
  between operations  0.64 us (1%)
    pallas_call x1, Pallas kernels, local(): pl.pallas_call(functools.partial(kernel, depth), out_shape=shapes, in_spe...  57.5 us
    pallas_call x1, Pallas kernels, local(): pl.pallas_call(settle, out_shape=shapes, in_specs=[vmem] * 3, out_specs=(...  1.38 us

profile of v2, /device:TPU:1, one launch (start us, length us, event | category | flops | bytes accessed | tf_op | source)
XLA Modules:
  0.0 59.5 jit_solution(17252173269772916532)
XLA Ops:
  0.6 57.5 %shard_map.157 = (f32[8,64]{1,0:T(8,128)}, f32[8,1024]{1,0:T(8,128)}, f32[8,64]{1,0:T(8,128)}) custom-call(bf16[8,128]{1,0:T(8,128)(2,1)} %tokens_hbm.1, f32[1,128]{1,0:T(1,128)} %bitcast.21, bf16[128,1536]{1,0:T(8,128)(2,1)} %ask_hbm.1, bf16[1088,128]{1,0:T(8,128)(2,1)} %bitcast.14, f32[12,128]{1,0:T(8,128)} %bitcast.19, f32[1,1024]{1,0:T(1,128)} %bitcast.20, ...), custom_call_target="tpu_custom_call" | custom-call | tf_op jit(solution)/shard_map/pallas_call | solution.py:431
  58.2 1.4 %shard_map.158 = (f32[8,64]{1,0:T(8,128)}, f32[8,1024]{1,0:T(8,128)}, f32[8,64]{1,0:T(8,128)}) custom-call(f32[8,64]{1,0:T(8,128)} %get-tuple-element.6.a, f32[8,1024]{1,0:T(8,128)} %get-tuple-element.7.b, f32[8,64]{1,0:T(8,128)} %get-tuple-element.8.c), custom_call_target="tpu_custom_call" | custom-call | tf_op jit(solution)/shard_map/pallas_call | solution.py:460

commit v3 on v2

--- a/solution.py
+++ b/solution.py
@@ -12,7 +12,7 @@
 THETA = 10000.0
 RING = 4
 MESH = pl.DeviceIdType.MESH
-PART, MID, FULL, ASK_Y, ASK_Z, MIX, MIX2, OUT, OUT2, PHASES = 0, 1, 2, 3, 8, 16, 24, 25, 26, 27
+PART, MID, FULL, ASK_Y, ASK_Z, MIX, MIX2, OUT, PHASES = 0, 1, 2, 3, 8, 16, 24, 25, 26
 F32 = jnp.float32
 BF16 = jnp.bfloat16
 
@@ -70,11 +70,10 @@
     mix2_recv,
     out_send,
     out_recv,
-    out2_send,
-    out2_recv,
     local_sem,
     sent_sems,
     come_sems,
+    greeted,
     lengths,
 ):
     kv = lax.axis_index("kv")
@@ -121,13 +120,47 @@
     plane = [(e, c) for e in (*order, 0) for c in range(2) if e or c]
 
     barrier = pltpu.get_barrier_semaphore()
+
+    def greet(device):
+        pl.semaphore_signal(barrier, inc=1, device_id=device, device_id_type=MESH)
+
+    for e in order:
+        greet(at(z, yp(e), 0))
     for d in near_first:
-        pl.semaphore_signal(barrier, inc=1, device_id=at(zp(d), y), device_id_type=MESH)
-    for e, c in plane:
+        greet(at(zp(d), y, 1))
+
+    @pl.when(tp == 0)
+    def _():
+        greet(at(z, y, 1))
+
+    @pl.when(tp == 1)
+    def _():
+        greet(at(z, y, 0))
+
+    def tell(which):
         pl.semaphore_signal(
-            barrier, inc=1, device_id=at(z, yp(e), (tp + c) % 2), device_id_type=MESH
+            greeted.at[which], inc=1, device_id=at(z, y, (tp + 1) % 2), device_id_type=MESH
         )
-    greeted = len(near_first) + len(plane)
+
+    def plane_is_here():
+        @pl.when(tp == 0)
+        def _():
+            pl.semaphore_wait(barrier, 2 * RING - 1)
+            tell(0)
+
+        @pl.when(tp == 1)
+        def _():
+            pl.semaphore_wait(greeted.at[0], 1)
+
+    def line_is_here():
+        @pl.when(tp == 1)
+        def _():
+            pl.semaphore_wait(barrier, 2 * depth - 1)
+            tell(1)
+
+        @pl.when(tp == 0)
+        def _():
+            pl.semaphore_wait(greeted.at[1], 1)
 
     loads = {}
 
@@ -173,7 +206,7 @@
     for t, tile in enumerate(tiles):
         part_send[t // 6, t // 3 % 2, t % 3] = tile
 
-    pl.semaphore_wait(barrier, greeted)
+    plane_is_here()
     for e in order:
         send(part_send.at[yp(e), tp], part_recv.at[e - 1], PART, PART, at(z, yp(e)))
 
@@ -199,6 +232,7 @@
     for e in range(RING - 1):
         total = total + part_recv[e]
     mid_recv[pl.ds(z, 1)] = total[None]
+    line_is_here()
     for d in near_first:
         send(mid_recv.at[z], mid_recv.at[z], MID, MID, at(zp(d), y))
     arrived(mid_recv.at[1:depth], MID)
@@ -347,30 +381,27 @@
 
     values = plain(attended, payload[...]).astype(BF16)
     projected = plain(values, w_out[...])
-    first = lane8 < 64
-    for i in range(depth // 2):
-        for j in range(RING):
-            a = 128 * (2 * i * RING + j)
-            b = 128 * ((2 * i + 1) * RING + j)
-            one, two = projected[:, a : a + 128], projected[:, b : b + 128]
-            out_send[j, 0, i] = jnp.where(first, one, pltpu.roll(two, 64, 1)).astype(BF16)
-            out_send[j, 1, i] = jnp.where(first, pltpu.roll(one, 64, 1), two).astype(BF16)
-    for e, c in plane:
-        core = (tp + c) % 2
-        theirs = out_recv.at[2 * e + c]
-        send(out_send.at[yp(e), core], theirs, OUT, OUT, at(z, yp(e), core))
-    found = out_send[y, tp].astype(F32)
-    arrived(out_recv.at[1 : 2 * RING], OUT)
-    for k in range(1, 2 * RING):
+    kept = (row8 < 4) == (lane8 < 64)
+    for k in range(RING * depth):
+        tile = projected[:, 128 * k : 128 * k + 128]
+        tile = jnp.where(kept, tile, pltpu.roll(pltpu.roll(tile, 64, 1), 4, 0)).astype(BF16)
+        out_send[k, 0] = tile[0:4]
+        out_send[k, 1] = tile[4:8]
+    slot = 0
+    for d in (*near_first, 0):
+        for e, c in (*plane, (0, 0)):
+            if d or e or c:
+                core = (tp + c) % 2
+                chip = zp(d) * RING + yp(e)
+                own, theirs = out_send.at[chip, core], out_recv.at[slot]
+                send(own, theirs, OUT, OUT, at(zp(d), yp(e), core))
+                slot += 1
+    found = out_send[kv, tp].astype(F32)
+    arrived(out_recv, OUT)
+    for k in range(slot):
         found = found + out_recv[k].astype(F32)
-    out2_send[...] = found.astype(BF16)
-    for d in near_first:
-        send(out2_send.at[zp(d) // 2], out2_recv.at[d], OUT2, OUT2, at(zp(d), y))
-    found = out2_send[z // 2].astype(F32)
-    arrived(out2_recv.at[1:depth], OUT2)
-    for d in range(1, depth):
-        found = found + out2_recv[d].astype(F32)
-    attention_out[...] = jnp.where(z % 2 == 0, found[:, 0:64], found[:, 64:128])
+    attention_out[0:4] = found[:, 0:64]
+    attention_out[4:8] = found[:, 64:128]
 
     for ref, phase in (
         (part_recv, PART),
@@ -380,8 +411,7 @@
         (queries.at[1:RING], ASK_Y),
         (mix_send, MIX),
         (mix2_recv.at[1:depth], MIX2),
-        (out_recv.at[1 : 2 * RING], OUT),
-        (out2_recv.at[1:depth], OUT2),
+        (out_recv, OUT),
     ):
         describe(ref, ref, phase, 0, at(z, y)).wait_send()
 
@@ -446,13 +476,12 @@
             pltpu.VMEM((8, RING - 1, depth, 1152), BF16),
             pltpu.VMEM((8, depth, 1152), F32),
             pltpu.VMEM((depth, 8, 1152), F32),
-            pltpu.VMEM((RING, 2, depth // 2, 8, 128), BF16),
-            pltpu.VMEM((2 * RING, depth // 2, 8, 128), BF16),
-            pltpu.VMEM((depth // 2, 8, 128), BF16),
-            pltpu.VMEM((depth, 8, 128), BF16),
+            pltpu.VMEM((RING * depth, 2, 4, 128), BF16),
+            pltpu.VMEM((2 * RING * depth - 1, 4, 128), BF16),
             dma((len(operands) + 1,)),
             dma((PHASES,)),
             dma((PHASES,)),
+            pltpu.SemaphoreType.REGULAR((2,)),
             pltpu.SMEM((8,), jnp.int32),
         ],
         compiler_params=pltpu.CompilerParams(collective_id=0, has_side_effects=True),

time: 59.7 us -> 56 us (0.938)
  Pallas kernels: 58.9 us -> 55.2 us
    pallas_call x1, Pallas kernels: 57.5 us -> 53.8 us  [local(): pl.pallas_call(functools.partial(kernel, depth), out_shape=shapes, in_spe...]
where the time goes in v3:
time: 56 us; the launch traced here: 55.9 us
  Pallas kernels  55.2 us (99%)
  between operations  0.64 us (1%)
    pallas_call x1, Pallas kernels, local(): pl.pallas_call(functools.partial(kernel, depth), out_shape=shapes, in_spe...  53.8 us
    pallas_call x1, Pallas kernels, local(): pl.pallas_call(settle, out_shape=shapes, in_specs=[vmem] * 3, out_specs=(...  1.38 us

profile of v3, /device:TPU:1, one launch (start us, length us, event | category | flops | bytes accessed | tf_op | source)
XLA Modules:
  0.0 55.9 jit_solution(9350393359440646538)
XLA Ops:
  0.6 53.8 %shard_map.157 = (f32[8,64]{1,0:T(8,128)}, f32[8,1024]{1,0:T(8,128)}, f32[8,64]{1,0:T(8,128)}) custom-call(bf16[8,128]{1,0:T(8,128)(2,1)} %tokens_hbm.1, f32[1,128]{1,0:T(1,128)} %bitcast.21, bf16[128,1536]{1,0:T(8,128)(2,1)} %ask_hbm.1, bf16[1088,128]{1,0:T(8,128)(2,1)} %bitcast.14, f32[12,128]{1,0:T(8,128)} %bitcast.19, f32[1,1024]{1,0:T(1,128)} %bitcast.20, ...), custom_call_target="tpu_custom_call" | custom-call | tf_op jit(solution)/shard_map/pallas_call | solution.py:461
  54.5 1.4 %shard_map.158 = (f32[8,64]{1,0:T(8,128)}, f32[8,1024]{1,0:T(8,128)}, f32[8,64]{1,0:T(8,128)}) custom-call(f32[8,64]{1,0:T(8,128)} %get-tuple-element.6.a, f32[8,1024]{1,0:T(8,128)} %get-tuple-element.7.b, f32[8,64]{1,0:T(8,128)} %get-tuple-element.8.c), custom_call_target="tpu_custom_call" | custom-call | tf_op jit(solution)/shard_map/pallas_call | solution.py:489

commit v4 on v3

--- a/solution.py
+++ b/solution.py
@@ -12,7 +12,7 @@
 THETA = 10000.0
 RING = 4
 MESH = pl.DeviceIdType.MESH
-PART, MID, FULL, ASK_Y, ASK_Z, MIX, MIX2, OUT, PHASES = 0, 1, 2, 3, 8, 16, 24, 25, 26
+PART, MID, FULL, ASK_Y, ASK_Z, MIX, MIX2, OUT, ASK_X, PHASES = 0, 1, 2, 3, 11, 27, 35, 36, 37, 38
 F32 = jnp.float32
 BF16 = jnp.bfloat16
 
@@ -80,8 +80,8 @@
     tp = lax.axis_index("tp")
     z, y = kv // RING, kv % RING
     span = 256
-    near_first = sorted(range(1, depth), key=lambda d: min(d, depth - d))
-    order = (1, 3, 2)
+    far_first = sorted(range(1, depth), key=lambda d: -min(d, depth - d))
+    order = (2, 1, 3)
 
     def at(zz, yy, cc=None):
         where = {"kv": zz * RING + yy}
@@ -126,7 +126,7 @@
 
     for e in order:
         greet(at(z, yp(e), 0))
-    for d in near_first:
+    for d in far_first:
         greet(at(zp(d), y, 1))
 
     @pl.when(tp == 0)
@@ -233,7 +233,7 @@
         total = total + part_recv[e]
     mid_recv[pl.ds(z, 1)] = total[None]
     line_is_here()
-    for d in near_first:
+    for d in far_first:
         send(mid_recv.at[z], mid_recv.at[z], MID, MID, at(zp(d), y))
     arrived(mid_recv.at[1:depth], MID)
     total = mid_recv[0]
@@ -254,17 +254,31 @@
     ask_gains = jnp.concatenate([ask_gain[t : t + 1] for t in range(12)], axis=1)
     squeezed = (query_down * lax.rsqrt(mean_square + EPS) * ask_gains).astype(BF16)
     nope = plain(squeezed, unspun[...]).astype(BF16)
-    turned = spinning(across(squeezed, spin[...])).astype(BF16)
-    queries[0, 0, :, 1024:1152] = turned
-    queries[0, 0, :, 0:1024] = plain(nope, lock[...]).astype(BF16)
-
-    def to_plane(d):
+    turned = spinning(across(squeezed, spin[...]))
+    absorbed = plain(nope, lock[...])
+    for h in range(2):
+        queries[h, 0, 0, :, 1024:1152] = turned[4 * h : 4 * h + 4].astype(BF16)
+        queries[h, 0, 0, :, 0:1024] = absorbed[4 * h : 4 * h + 4].astype(BF16)
+
+    def to_plane(h, d):
         for e in order:
-            send(queries.at[0, d], queries.at[e, d], ASK_Y, ASK_Y + e, at(z, yp(e)))
-
-    for d in near_first:
-        send(queries.at[0, 0], queries.at[0, d], ASK_Z, ASK_Z + d, at(zp(d), y))
-    to_plane(0)
+            if h and d and e == 2:
+                continue
+            come = ASK_X if h and e == 2 else ASK_Y + RING * h + e
+            send(queries.at[h, 0, d], queries.at[h, e, d], ASK_Y, come, at(z, yp(e)))
+
+    def to_line(h, e):
+        for d in far_first:
+            if e:
+                come = ASK_Y + RING * h + e
+            else:
+                come = ASK_Z + depth * h + d
+            send(queries.at[h, e, 0], queries.at[h, e, d], ASK_Z, come, at(zp(d), y))
+
+    to_line(0, 0)
+    to_plane(0, 0)
+    to_plane(1, 0)
+    to_line(1, 0)
 
     hidden_down = jnp.concatenate([full[t // 3, t % 3] for t in range(12, 20)], axis=1) * row_scale
     mean_square = jnp.mean(hidden_down * hidden_down, axis=1, keepdims=True)
@@ -281,7 +295,8 @@
     spun_columns = across(eye, incoming_spun.astype(BF16))
     position_row = kv * span + lax.broadcasted_iota(jnp.int32, (64, span), 1)
     position_column = kv * span + lax.broadcasted_iota(jnp.int32, (span, 1024), 0)
-    for s in range(8):
+
+    def renew(s):
         rotary[s] = jnp.where(
             position_row == lengths[s], spun_columns[:, s : s + 1], rotary[s].astype(F32)
         ).astype(BF16)
@@ -290,24 +305,29 @@
             incoming_hidden[s : s + 1],
             latent[span * s : span * s + span].astype(F32),
         ).astype(BF16)
-        if s < depth - 1:
-            d = near_first[s]
-            arrived(queries.at[0, d], ASK_Z + d)
-            to_plane(d)
-
-    group = 8 * depth
+
+    stale = list(range(8))
+    for h in range(2):
+        for d in far_first:
+            if stale:
+                renew(stale.pop(0))
+            arrived(queries.at[h, 0, d], ASK_Z + depth * h + d)
+            to_plane(h, d)
+            if h == 0 and d == far_first[4]:
+                arrived(queries.at[1, 2, 0], ASK_X)
+                to_line(1, 2)
+
+    group = 4 * depth
     come = lax.broadcasted_iota(jnp.int32, (group, group), 1)
     went = lax.broadcasted_iota(jnp.int32, (group, group), 0)
-    shuffle = (come == went % depth * 8 + went // depth).astype(BF16)
-
-    def sort_rows(e):
-        found = plain(shuffle, queries[e].reshape(group, 1152)).astype(BF16)
-        sorted_queries[:, e] = found.reshape(8, depth, 1152)
-
-    sort_rows(0)
-    for e in order:
-        arrived(queries.at[e], ASK_Y + e)
-        sort_rows(e)
+    shuffle = (come == went % depth * 4 + went // depth).astype(BF16)
+
+    def sort_rows(h, e):
+        found = plain(shuffle, queries[h, e].reshape(group, 1152)).astype(BF16)
+        sorted_queries[4 * h : 4 * h + 4, e] = found.reshape(4, depth, 1152)
+
+    sort_rows(0, 0)
+    sort_rows(1, 0)
 
     heads = RING * depth
     position = kv * span + lax.broadcasted_iota(jnp.int32, (heads, span), 1)
@@ -344,11 +364,15 @@
         for e in order:
             send(mix_send.at[s, e - 1], mix_recv.at[s, e - 1], MIX, MIX + s, at(z, ym(e)))
 
-    found = {0: score(0)}
-    for s in range(8):
-        if s < 7:
-            found[s + 1] = score(s + 1)
-        mix(s, *soften(s, found.pop(s)))
+    for h in range(2):
+        for e in order:
+            arrived(queries.at[h, e, int(h == 1 and e == 2) :], ASK_Y + RING * h + e)
+            sort_rows(h, e)
+        found = {4 * h: score(4 * h)}
+        for s in range(4 * h, 4 * h + 4):
+            if s < 4 * h + 3:
+                found[s + 1] = score(s + 1)
+            mix(s, *soften(s, found.pop(s)))
 
     def combine(parts):
         tops = [p[:, 1024:1025] + p[:, 1025:1026] for p in parts]
@@ -368,7 +392,7 @@
         mix2_send[s, :, 1024:1152] = jnp.where(
             lane8k == 0, top, jnp.where(lane8k == 2, total, 0.0)
         )
-        for d in near_first:
+        for d in far_first:
             own, theirs = mix2_send.at[s, pl.ds(d, 1)], mix2_recv.at[d, pl.ds(s, 1)]
             send(own, theirs, MIX2, MIX2, at(zm(d), y))
         mix2_recv[0, s : s + 1] = mix2_send[s, 0:1]
@@ -388,7 +412,7 @@
         out_send[k, 0] = tile[0:4]
         out_send[k, 1] = tile[4:8]
     slot = 0
-    for d in (*near_first, 0):
+    for d in (*far_first, 0):
         for e, c in (*plane, (0, 0)):
             if d or e or c:
                 core = (tp + c) % 2
@@ -407,8 +431,11 @@
         (part_recv, PART),
         (mid_recv.at[1:depth], MID),
         (full.at[1 : 2 * RING], FULL),
-        (queries.at[0, 1:depth], ASK_Z),
-        (queries.at[1:RING], ASK_Y),
+        (queries.at[:, 0, 1:depth], ASK_Z),
+        (queries.at[1, 2, 1:depth], ASK_Z),
+        (queries.at[0, 1:RING], ASK_Y),
+        (queries.at[1, 0:2], ASK_Y),
+        (queries.at[1, 0, 0], ASK_Y),
         (mix_send, MIX),
         (mix2_recv.at[1:depth], MIX2),
         (out_recv, OUT),
@@ -469,7 +496,7 @@
             pltpu.VMEM((RING - 1, 3, 8, 128), F32),
             pltpu.VMEM((depth, 3, 8, 128), F32),
             pltpu.VMEM((2 * RING, 3, 8, 128), F32),
-            pltpu.VMEM((RING, depth, 8, 1152), BF16),
+            pltpu.VMEM((2, RING, depth, 4, 1152), BF16),
             pltpu.VMEM((8, RING, depth, 1152), BF16),
             pltpu.VMEM((8, depth, 1152), F32),
             pltpu.VMEM((8, RING - 1, depth, 1152), BF16),

time: 56 us -> 52.9 us (0.945)
  Pallas kernels: 55.2 us -> 52.1 us
    pallas_call x1, Pallas kernels: 53.8 us -> 50.7 us  [local(): pl.pallas_call(functools.partial(kernel, depth), out_shape=shapes, in_spe...]
where the time goes in v4:
time: 52.9 us; the launch traced here: 52.7 us
  Pallas kernels  52.1 us (98%)
  between operations  0.64 us (1%)
    pallas_call x1, Pallas kernels, local(): pl.pallas_call(functools.partial(kernel, depth), out_shape=shapes, in_spe...  50.7 us
    pallas_call x1, Pallas kernels, local(): pl.pallas_call(settle, out_shape=shapes, in_specs=[vmem] * 3, out_specs=(...  1.38 us

profile of v4, /device:TPU:1, one launch (start us, length us, event | category | flops | bytes accessed | tf_op | source)
XLA Modules:
  0.0 52.7 jit_solution(12674867889003522205)
XLA Ops:
  0.6 50.7 %shard_map.157 = (f32[8,64]{1,0:T(8,128)}, f32[8,1024]{1,0:T(8,128)}, f32[8,64]{1,0:T(8,128)}) custom-call(bf16[8,128]{1,0:T(8,128)(2,1)} %tokens_hbm.1, f32[1,128]{1,0:T(1,128)} %bitcast.21, bf16[128,1536]{1,0:T(8,128)(2,1)} %ask_hbm.1, bf16[1088,128]{1,0:T(8,128)(2,1)} %bitcast.14, f32[12,128]{1,0:T(8,128)} %bitcast.19, f32[1,1024]{1,0:T(1,128)} %bitcast.20, ...), custom_call_target="tpu_custom_call" | custom-call | tf_op jit(solution)/shard_map/pallas_call | solution.py:488
  51.4 1.4 %shard_map.158 = (f32[8,64]{1,0:T(8,128)}, f32[8,1024]{1,0:T(8,128)}, f32[8,64]{1,0:T(8,128)}) custom-call(f32[8,64]{1,0:T(8,128)} %get-tuple-element.6.a, f32[8,1024]{1,0:T(8,128)} %get-tuple-element.7.b, f32[8,64]{1,0:T(8,128)} %get-tuple-element.8.c), custom_call_target="tpu_custom_call" | custom-call | tf_op jit(solution)/shard_map/pallas_call | solution.py:516

commit v5 on v4

--- a/solution.py
+++ b/solution.py
@@ -13,6 +13,7 @@
 RING = 4
 MESH = pl.DeviceIdType.MESH
 PART, MID, FULL, ASK_Y, ASK_Z, MIX, MIX2, OUT, ASK_X, PHASES = 0, 1, 2, 3, 11, 27, 35, 36, 37, 38
+SENT = (PART, MID, FULL, ASK_Y, ASK_Z, MIX, MIX2, OUT)
 F32 = jnp.float32
 BF16 = jnp.bfloat16
 
@@ -105,7 +106,7 @@
         return pltpu.make_async_remote_copy(
             src_ref=src,
             dst_ref=dst,
-            send_sem=sent_sems.at[phase],
+            send_sem=sent_sems.at[SENT.index(phase)],
             recv_sem=come_sems.at[arrival],
             device_id=device,
             device_id_type=MESH,
@@ -506,7 +507,7 @@
             pltpu.VMEM((RING * depth, 2, 4, 128), BF16),
             pltpu.VMEM((2 * RING * depth - 1, 4, 128), BF16),
             dma((len(operands) + 1,)),
-            dma((PHASES,)),
+            dma((len(SENT),)),
             dma((PHASES,)),
             pltpu.SemaphoreType.REGULAR((2,)),
             pltpu.SMEM((8,), jnp.int32),

time: 52.9 us -> 52.6 us (level)
  no operation moved by 1% of the time
where the time goes in v5:
time: 52.6 us; the launch traced here: 52.5 us
  Pallas kernels  51.8 us (98%)
  between operations  0.64 us (1%)
    pallas_call x1, Pallas kernels, local(): pl.pallas_call(functools.partial(kernel, depth), out_shape=shapes, in_spe...  50.4 us
    pallas_call x1, Pallas kernels, local(): pl.pallas_call(settle, out_shape=shapes, in_specs=[vmem] * 3, out_specs=(...  1.38 us

profile of v5, /device:TPU:1, one launch (start us, length us, event | category | flops | bytes accessed | tf_op | source)
XLA Modules:
  0.0 52.5 jit_solution(4320705175520297333)
XLA Ops:
  0.6 50.4 %shard_map.157 = (f32[8,64]{1,0:T(8,128)}, f32[8,1024]{1,0:T(8,128)}, f32[8,64]{1,0:T(8,128)}) custom-call(bf16[8,128]{1,0:T(8,128)(2,1)} %tokens_hbm.1, f32[1,128]{1,0:T(1,128)} %bitcast.21, bf16[128,1536]{1,0:T(8,128)(2,1)} %ask_hbm.1, bf16[1088,128]{1,0:T(8,128)(2,1)} %bitcast.14, f32[12,128]{1,0:T(8,128)} %bitcast.19, f32[1,1024]{1,0:T(1,128)} %bitcast.20, ...), custom_call_target="tpu_custom_call" | custom-call | tf_op jit(solution)/shard_map/pallas_call | solution.py:489
  51.1 1.4 %shard_map.158 = (f32[8,64]{1,0:T(8,128)}, f32[8,1024]{1,0:T(8,128)}, f32[8,64]{1,0:T(8,128)}) custom-call(f32[8,64]{1,0:T(8,128)} %get-tuple-element.6.a, f32[8,1024]{1,0:T(8,128)} %get-tuple-element.7.b, f32[8,64]{1,0:T(8,128)} %get-tuple-element.8.c), custom_call_target="tpu_custom_call" | custom-call | tf_op jit(solution)/shard_map/pallas_call | solution.py:517
